TPU v7x, 128 devices: a whole 4x4x4 slice. The times are simulated.
128 devices in a mesh: sp: 16 (over z, y), tp: 8 (over x, core).
Axes of the slice: x: 4, y: 4, z: 4, core: 2. Of those that a mesh axis runs over, the one named last changes fastest.
Arguments:
- inputs: bfloat16 [8192, 4096], P(('sp', 'tp')), may hold values from -42 to 42
- a_query_w: bfloat16 [4096, 2048], P(None, 'tp'), may hold values from -0.12570312 to 0.12570312
- a_key_w: bfloat16 [4096, 2048], P(None, 'tp'), may hold values from -0.12570312 to 0.12570312
- a_value_w: bfloat16 [4096, 2048], P(None, 'tp'), may hold values from -0.09375 to 0.09375
- b_query_w: bfloat16 [4096, 2048], P(None, 'tp'), may hold values from -0.12570312 to 0.12570312
- b_key_w: bfloat16 [4096, 512], P(None, 'tp'), may hold values from -0.12570312 to 0.12570312
- b_value_w: bfloat16 [4096, 512], P(None, 'tp'), may hold values from -0.09375 to 0.09375
- head_lambda: float32 [16], P('tp'), may hold values from 0.3 to 0.8
- head_gain: float32 [128], replicated, may hold values from 0.1 to 1.9
- sink_logit: float32 [32], P('tp'), may hold values from 2 to 7
- a_out_w: bfloat16 [2048, 4096], P('tp'), may hold values from -0.125 to 0.125
- b_out_w: bfloat16 [2048, 4096], P('tp'), may hold values from -0.625 to 0.625
Outputs:
- mixed: bfloat16 [8192, 4096], P(('sp', 'tp'))
All inputs are finite; a program needn't handle non-finite values.
Results may differ from a plain program's by a relative error of at most 0.015.
Values may be sent and summed in bfloat16 or wider, within the bound.
A program may use at most 128 MiB of HBM per device.

v0:
```python
import math
import jax
import jax.numpy as jnp
from jax import lax
from jax.sharding import PartitionSpec as P

HEAD_DIM = 64
VALUE_DIM = 128
WINDOW = 128
norm_eps = 0.0001
head_scale = 0.8
mask_fill = -1e30


def from_behind(value, axis, by):
    size = lax.axis_size(axis)
    pairs = [(i, i + by) for i in range(size) if 0 <= i + by < size]
    return lax.ppermute(value, axis, pairs)


def side_by_side(arrays, axis, dim, along):
    widths = [a.shape[along] for a in arrays]
    both = jnp.concatenate(arrays, axis=along)
    whole = lax.all_gather(both, axis, axis=dim, tiled=True)
    return tuple(jnp.split(whole, [sum(widths[:k]) for k in range(1, len(widths))], axis=along))


def key_span(row_count):
    span_rows = math.gcd(row_count, 1024)
    return span_rows


def attend_block(carried, queries, query_pos, block_keys, block_values, key_pos):
    running, totals, numerator = carried
    scores = jnp.einsum(
        "qhmd,khmd->hmqk", queries, block_keys, preferred_element_type=jnp.float32
    ) * HEAD_DIM ** (-0.5)
    allowed = query_pos[:, None] >= key_pos[None, :]
    scores = jnp.where(allowed, scores, mask_fill)
    updated = jnp.maximum(running, jnp.max(scores, axis=-1))
    weights = jnp.where(allowed, jnp.exp(scores - updated[..., None]), 0.0)
    shrink = jnp.exp(running - updated)
    totals = totals * shrink + jnp.sum(weights, axis=-1)
    numerator = numerator * shrink[..., None] + jnp.einsum(
        "hmqk,khe->hmqe",
        weights.astype(jnp.bfloat16),
        block_values,
        preferred_element_type=jnp.float32,
    )
    return (updated, totals, numerator)


def advance(states, groups, key_rows, value_rows):
    row_count = key_rows.shape[0]
    span_rows = key_span(row_count)
    local_heads = value_rows.shape[1] // VALUE_DIM
    key_rows = key_rows.reshape(row_count, local_heads, 2, HEAD_DIM)
    value_rows = value_rows.reshape(row_count, local_heads, VALUE_DIM)

    def one_span(span_index, current):
        span_start = span_index * span_rows
        block_keys = lax.dynamic_slice_in_dim(key_rows, span_start, span_rows, 0)
        block_values = lax.dynamic_slice_in_dim(value_rows, span_start, span_rows, 0)
        key_pos = span_start + jnp.arange(span_rows, dtype=jnp.int32)
        results = []
        for query_group, carried in zip(groups, current):
            queries, query_pos = query_group

            def compute(given_state, queries=queries, query_pos=query_pos):
                return attend_block(
                    given_state, queries, query_pos, block_keys, block_values, key_pos
                )

            def unchanged(given_state):
                return given_state

            results.append(lax.cond(key_pos[0] <= query_pos[-1], compute, unchanged, carried))
        return tuple(results)

    return lax.fori_loop(0, row_count // span_rows, one_span, states)


def finish_heads(carried, head_lambda, head_gain):
    running, totals, numerator = carried
    means = numerator / totals[..., None]
    difference = means[:, 0] - head_lambda[:, None, None] * means[:, 1]
    mean_square = jnp.mean(difference * difference, axis=-1, keepdims=True)
    return (difference * lax.rsqrt(mean_square + norm_eps) * head_gain * head_scale).astype(
        jnp.bfloat16
    )


def shards(
    inputs,
    a_query_w,
    a_key_w,
    a_value_w,
    b_query_w,
    b_key_w,
    b_value_w,
    head_lambda,
    head_gain,
    sink_logit,
    a_out_w,
    b_out_w,
):
    matrices = (a_query_w, a_key_w, a_value_w, b_query_w, b_key_w, b_value_w)

    def project(shard_piece):
        return jnp.concatenate(
            [
                jnp.dot(shard_piece, matrix, preferred_element_type=jnp.float32).astype(
                    jnp.bfloat16
                )
                for matrix in matrices
            ],
            axis=1,
        )

    projected = project(lax.all_gather(inputs, "tp", axis=0, tiled=True))
    seg_rows = projected.shape[0]
    column_edges = [0]
    for matrix in matrices:
        column_edges.append(column_edges[-1] + matrix.shape[1])
    a_query = projected[:, column_edges[0] : column_edges[1]]
    a_key = projected[:, column_edges[1] : column_edges[2]]
    a_value = projected[:, column_edges[2] : column_edges[3]]
    b_query = projected[:, column_edges[3] : column_edges[4]]
    b_pair = projected[:, column_edges[4] : column_edges[6]]
    local_heads = head_lambda.shape[0]
    offset = lax.axis_index("sp") * seg_rows
    positions = offset + jnp.arange(seg_rows, dtype=jnp.int32)
    query_heads = a_query.reshape(seg_rows, local_heads, 2, HEAD_DIM)
    groups = ((query_heads, positions),)
    initial = tuple(
        (
            (
                jnp.full((local_heads, 2, group_queries.shape[0]), mask_fill, jnp.float32),
                jnp.zeros((local_heads, 2, group_queries.shape[0]), jnp.float32),
                jnp.zeros((local_heads, 2, group_queries.shape[0], VALUE_DIM), jnp.float32),
            )
            for group_queries, group_pos in groups
        )
    )
    earlier = from_behind(b_pair[seg_rows - WINDOW :], "sp", 1)
    shard_piece = side_by_side((a_key, a_value), "sp", 0, 1)
    states = advance(initial, groups, shard_piece[0], shard_piece[1])
    finished = [finish_heads(carried, head_lambda, head_gain) for carried in states]
    a_heads = finished[0]
    kv_heads = b_pair.shape[1] // (2 * HEAD_DIM)
    group_size = b_query.shape[1] // HEAD_DIM // kv_heads
    extended = jnp.concatenate([earlier, b_pair], axis=0)
    near_keys = extended[:, : kv_heads * HEAD_DIM].reshape(WINDOW + seg_rows, kv_heads, HEAD_DIM)
    near_values = extended[:, kv_heads * HEAD_DIM :].reshape(WINDOW + seg_rows, kv_heads, HEAD_DIM)
    window_queries = b_query.reshape(seg_rows, kv_heads, group_size, HEAD_DIM)
    sink_term = sink_logit.reshape(kv_heads, group_size)[:, :, None]
    query_span = math.gcd(seg_rows, 512)
    scores = jnp.einsum(
        "qhgd,khd->hgqk", window_queries, near_keys, preferred_element_type=jnp.float32
    ) * HEAD_DIM ** (-0.5)
    query_pos = offset + 0 + jnp.arange(query_span, dtype=jnp.int32)
    near_pos = offset + 0 - WINDOW + jnp.arange(query_span + WINDOW, dtype=jnp.int32)
    distance = query_pos[:, None] - near_pos[None, :]
    allowed = (distance >= 0) & (distance < WINDOW) & (near_pos[None, :] >= 0)
    scores = jnp.where(allowed, scores, mask_fill)
    row_top = jnp.maximum(jnp.max(scores, axis=-1), sink_term)
    weights = jnp.where(allowed, jnp.exp(scores - row_top[..., None]), 0.0)
    row_total = jnp.sum(weights, axis=-1) + jnp.exp(sink_term - row_top)
    probs = (weights / row_total[..., None]).astype(jnp.bfloat16)
    block_out = jnp.einsum("hgqk,khd->qhgd", probs, near_values, preferred_element_type=jnp.float32)
    outputs = block_out.astype(jnp.bfloat16).reshape(query_span, kv_heads * group_size * HEAD_DIM)
    a_weight = a_out_w.reshape(local_heads, VALUE_DIM, a_out_w.shape[1])
    return lax.psum_scatter(
        (
            jnp.einsum("hqe,hen->qn", a_heads, a_weight, preferred_element_type=jnp.float32)
            + jnp.dot(outputs, b_out_w, preferred_element_type=jnp.float32)
        ).astype(jnp.bfloat16),
        "tp",
        scatter_dimension=0,
        tiled=True,
    )


def solution(mesh):
    return jax.shard_map(
        shards,
        mesh=mesh,
        in_specs=(
            P(("sp", "tp"), None),
            P(None, "tp"),
            P(None, "tp"),
            P(None, "tp"),
            P(None, "tp"),
            P(None, "tp"),
            P(None, "tp"),
            P("tp"),
            P(),
            P("tp"),
            P("tp", None),
            P("tp", None),
        ),
        out_specs=P(("sp", "tp"), None),
        check_vma=False,
    )
```

profile of v0, /device:TPU:0, one launch (start us, length us, event | category | flops | bytes accessed | tf_op | source)
XLA Modules:
  0.0 288.8 jit_solution(3257539258130049300)
XLA Ops:
  6.5 0.7 all-gather.3.cloned.1.call-update
  7.3 36.3 %all-gather.3.cloned.1.call-done = bf16[512,4096]{1,0:T(8,128)(2,1)} async-done(((bf16[64,4096]{1,0:T(8,128)(2,1)}), bf16[512,4096]{1,0:T(8,128)(2,1)}) %all-gather.3.cloned.1.call-update) | async-done | bytes 4194320 | tf_op jit(solution)/shard_map/all_gather | solution.py:120
  43.6 4.3 %convolution_convert_fusion.2 = bf16[512,256]{0,1:T(8,128)(2,1)S(1)} fusion(bf16[512,4096]{1,0:T(8,128)(2,1)} %all-gather.3.cloned.1.call-done, bf16[4096,256]{1,0:T(8,128)(2,1)} %param.19), kind=kOutput, calls=%fused_computation.37 | convolution fusion | flops 1073872896 | bytes 6553600 | tf_op jit(solution)/shard_map/dot_general | solution.py:112
  47.9 0.4 copy-done.9
  48.3 1.3 convolution_convert_fusion.3
  49.6 0.8 pad_maximum_fusion
  50.6 0.4 fusion.24
  51.0 3.8 %convolution_convert_fusion.4 = bf16[512,64]{0,1:T(8,128)(2,1)S(1)} fusion(bf16[512,4096]{1,0:T(8,128)(2,1)} %all-gather.3.cloned.1.call-done, bf16[4096,64]{0,1:T(8,128)(2,1)S(1)} %copy-done.4), kind=kOutput, calls=%fused_computation.39 | convolution fusion | flops 268468224 | bytes 4784128 | tf_op jit(solution)/shard_map/dot_general | solution.py:112
  54.9 1.4 convolution_convert_fusion.5
  56.3 3.5 %collective-permute-start = (bf16[128,128]{0,1:T(8,128)(2,1)S(1)}, bf16[128,128]{0,1:T(8,128)(2,1)S(1)}, u32[]{:S(2)}, u32[]{:S(2)}) collective-permute-start(bf16[128,128]{0,1:T(8,128)(2,1)S(1)} %pad_maximum_fusion.1), channel_id=1, source_target_pairs={{0,8},{8,16},{16,24},{24,32},{32,40},{40,48},{48,56},{56,64},{64,7... | collective-permute-start | bytes 98312 | tf_op jit(solution)/shard_map/ppermute | solution.py:18
  59.8 1.3 convolution_convert_fusion
  61.2 2.0 convolution_convert_fusion.1
  63.2 1.0 fusion.19
  64.3 0.1 broadcast_maximum_fusion
  64.3 1.3 fusion.20
  65.6 0.1 exponential_add_fusion
  65.7 1.8 fusion.25
  67.6 60.4 %all-gather.5.cloned.1.call-done = bf16[8192,512]{0,1:T(8,128)(2,1)} async-done(((bf16[512,512]{0,1:T(8,128)(2,1)}), bf16[8192,512]{0,1:T(8,128)(2,1)}) %all-gather.5.cloned.1.call-update) | async-done | bytes 8388624 | tf_op jit(solution)/shard_map/all_gather | solution.py:24
  128.0 5.9 %fusion.40 = (bf16[8192,256]{0,1:T(8,128)(2,1)}, bf16[8192,256]{0,1:T(8,128)(2,1)}) fusion(bf16[8192,512]{0,1:T(8,128)(2,1)} %all-gather.5.cloned.1.call-done), kind=kLoop, calls=%fused_computation.68 | loop fusion | bytes 16777216 | tf_op jit(solution)/shard_map/split | solution.py:25
  133.9 6.3 %copy.14 = bf16[8192,2,128]{2,0,1:T(8,128)(2,1)} copy(bf16[8192,2,128]{0,2,1:T(8,128)(2,1)} %bitcast.105) | data formatting | bytes 8388608 | tf_op jit(solution)/shard_map/while | solution.py:80
  140.3 31.0 %while.17 = (s32[]{:T(128)}, f32[2,2,512]{2,1,0:T(2,128)S(1)}, f32[2,2,512]{2,1,0:T(2,128)S(1)}, f32[2,2,512,128]{3,2,1,0:T(8,128)S(1)}, s32[512]{0:T(512)S(1)},...) while((s32[]{:T(128)}, f32[2,2,512]{2,1,0:T(2,128)S(1)}, ...), condition=%wide.region_5.6_spmd, body=%wide.region_0.5_spmd.sunk | while | flops 833623040 | bytes 30812476 | solution.py:80
  140.3 0.6 slice.65
  141.0 0.6 slice.64
  142.9 9.8 %conditional.2 = ((f32[2,2,512]{2,1,0:T(2,128)S(1)}, f32[2,2,512]{2,1,0:T(2,128)S(1)}, f32[2,2,512,128]{3,2,1,0:T(8,128)S(1)})) conditional(s32[]{:T(128)} %bitcast.103, (f32[2,2,512]{2,1,0:T(2,128)S(1)}, f32[2,2,512]{2,1,0:T(2,128)S(1)}, f32[2,2,512,128]{3,2,1,0:T(8,128)S(1)}) %tuple.51, (s32[512]{0:T(512)S(1)}, s32[1024]{0:T(1024)S(1)}, s32[]{:T(128)}, ...), branch_computations={%region_1.0_spmd, %region_2.4_spmd} | conditional | flops 833622016 | bytes 30808138 | solution.py:77
  143.0 0.4 broadcast_compare_fusion
  143.3 2.7 fusion
  146.1 2.1 fusion.2
  148.2 4.5 %fusion.6 = f32[2,2,512,128]{3,2,1,0:T(8,128)S(1)} fusion(f32[2,2,1024,512]{3,2,1,0:T(8,128)S(1)} %get-tuple-element.290, f32[2,2,512]{2,1,0:T(2,128)S(1)} %max.21, pred[512,1024]{0,1:T(8,128)(4,1)S(1)} %broadcast_compare_fusion, f32[2,2,512,128]{3,2,1,0:T(8,128)S(1)} %get-tuple-element.245, bf16[8192,2,128]{2,0,1:T(8,128)(2,1)} %get-tuple-element.246, ...), kind=kOutput, calls=%fused_computation.7 | convolution fusion | flops 547880960 | bytes 11550724 | tf_op jit(solution)/shard_map/while/body/eval_jaxpr/cond/branch_1_fun/hmqk,khe->hmqe/dot_general | solution.py:44
  152.7 0.6 slice.65
  153.4 0.6 slice.64
  155.4 0.6 slice.65
  156.0 0.6 slice.64
  158.1 0.6 slice.65
  158.7 0.6 slice.64
  160.7 0.6 slice.65
  161.4 0.6 slice.64
  163.4 0.6 slice.65
  164.0 0.6 slice.64
  166.0 0.6 slice.65
  166.7 0.6 slice.64
  168.7 0.6 slice.65
  169.3 0.6 slice.64
  171.3 0.3 broadcast_divide_fusion
  171.7 0.3 multiply_reduce_fusion
  172.0 1.3 fusion.30
  173.3 0.3 copy-done.3
  173.6 3.3 %fusion.18 = bf16[512,4096]{1,0:T(8,128)(2,1)} fusion(f32[512,4096,1]{1,0,2:T(8,128)S(1)} %fusion.30, bf16[512,256]{0,1:T(8,128)(2,1)S(1)} %bitcast.107, bf16[256,4096]{1,0:T(8,128)(2,1)S(1)} %copy-done.3), kind=kOutput, calls=%fused_computation.22 | convolution fusion | flops 1077936128 | bytes 14942208 | tf_op jit(solution)/shard_map/dot_general | solution.py:176
  176.9 105.4 %reduce-scatter.2.cloned.1.call-done = bf16[64,4096]{1,0:T(8,128)(2,1)} async-done(((bf16[512,4096]{1,0:T(8,128)(2,1)}), bf16[64,4096]{1,0:T(8,128)(2,1)}) %reduce-scatter.2.cloned.1.call-update) | async-done | bytes 524304 | tf_op jit(solution)/shard_map/reduce_scatter | solution.py:173
  (55 shorter events, 0.4 us)
Async XLA Ops:
  6.5 165.5 %copy-start = (bf16[256,4096]{1,0:T(8,128)(2,1)S(1)}, bf16[256,4096]{1,0:T(8,128)(2,1)}, u32[]{:S(2)}) copy-start(bf16[256,4096]{1,0:T(8,128)(2,1)} %param.26) | copy-start | bytes 6291460
  6.5 37.0 %all-gather.3.cloned.1.call-start = ((), (), s32[]{:S(2)}) async-start(), calls=%async_computation.1 | async-start | bytes 4718592 | tf_op jit(solution)/shard_map/all_gather | solution.py:120
  7.3 120.7 %all-gather.5.cloned.1.call-start = ((), (), s32[]{:S(2)}) async-start(), calls=%async_computation.2 | async-start | bytes 8912896 | tf_op jit(solution)/shard_map/all_gather | solution.py:24
  43.6 4.3 %copy-start.1 = (bf16[512,4096]{1,0:T(8,128)(2,1)S(1)}, bf16[512,4096]{1,0:T(8,128)(2,1)}, u32[]{:S(2)}) copy-start(bf16[512,4096]{1,0:T(8,128)(2,1)} %all-gather.3.cloned.1.call-done) | copy-start | bytes 12582916
  43.6 4.7 %copy-start.9 = (bf16[4096,256]{1,0:T(8,128)(2,1)S(1)}, bf16[4096,256]{1,0:T(8,128)(2,1)}, u32[]{:S(2)}) copy-start(bf16[4096,256]{1,0:T(8,128)(2,1)} %param.18) | copy-start | bytes 6291460
  48.3 2.7 copy-start.4
  49.6 5.2 %copy-start.5 = (bf16[4096,64]{0,1:T(8,128)(2,1)S(1)}, bf16[4096,64]{0,1:T(8,128)(2,1)}, u32[]{:S(2)}) copy-start(bf16[4096,64]{0,1:T(8,128)(2,1)} %param.21) | copy-start | bytes 1572868
  50.5 231.8 %reduce-scatter.2.cloned.1.call-start = ((), (), s32[]{:S(2)}) async-start(), calls=%async_computation.3 | async-start | bytes 4718592 | tf_op jit(solution)/shard_map/reduce_scatter | solution.py:173
  50.5 4.3 %copy-start.2 = (bf16[512,4096]{1,0:T(8,128)(2,1)S(1)}, bf16[512,4096]{1,0:T(8,128)(2,1)}, u32[]{:S(2)}) copy-start(bf16[512,4096]{1,0:T(8,128)(2,1)} %all-gather.3.cloned.1.call-done) | copy-start | bytes 12582916
  51.0 8.8 %copy-start.10 = (bf16[4096,256]{1,0:T(8,128)(2,1)S(1)}, bf16[4096,256]{1,0:T(8,128)(2,1)}, u32[]{:S(2)}) copy-start(bf16[4096,256]{1,0:T(8,128)(2,1)} %param.20) | copy-start | bytes 6291460
  56.3 4.9 %copy-start.11 = (bf16[4096,256]{1,0:T(8,128)(2,1)S(1)}, bf16[4096,256]{1,0:T(8,128)(2,1)}, u32[]{:S(2)}) copy-start(bf16[4096,256]{1,0:T(8,128)(2,1)} %param.17) | copy-start | bytes 6291460
  56.3 6.9 %collective-permute-start = (bf16[128,128]{0,1:T(8,128)(2,1)S(1)}, bf16[128,128]{0,1:T(8,128)(2,1)S(1)}, u32[]{:S(2)}, u32[]{:S(2)}) collective-permute-start(bf16[128,128]{0,1:T(8,128)(2,1)S(1)} %pad_maximum_fusion.1), channel_id=1, source_target_pairs={{0,8},{8,16},{16,24},{24,32},{32,40},{40,48},{48,56},{56,64},{64,7... | collective-permute-start | bytes 98312 | tf_op jit(solution)/shard_map/ppermute | solution.py:18
  63.2 1.1 copy-start.8
  140.3 31.4 %copy-start.6 = (f32[2]{0:T(128)S(1)}, f32[2]{0:T(128)}, u32[]{:S(2)}) copy-start(f32[2]{0:T(128)} %param.23) | copy-start | bytes 28
  140.3 31.7 %copy-start.7 = (f32[128]{0:T(128)S(1)}, f32[128]{0:T(128)}, u32[]{:S(2)}) copy-start(f32[128]{0:T(128)} %param.24) | copy-start | bytes 1540
  172.0 1.6 copy-start.3
Sparse Core Ops, SparseCore 0:
  9.0 34.4 all-gather.2
  50.6 77.3 all-gather.4
  177.0 105.1 reduce-scatter.1
where the time goes:
time: 290 us; the launch traced here: 289 us
  waiting for transfers between devices  203 us (70%)
  matrix products  28.8 us (10%)
  local copies, waits for them, and re-layouts  23 us (8%)
  between operations  13.4 us (5%)
  loops' own time  11.3 us (4%)
  other arithmetic  5.89 us (2%)
  starting transfers between devices  3.61 us (1%)
    reduce_scatter x1, waiting for transfers between devices, shards(): lax.psum_scatter((jnp.einsum('hqe,hen->qn', a_heads, a_weight, preferred_...  105 us
    all_gather x1, waiting for transfers between devices, side_by_side(): whole = lax.all_gather(both, axis, axis=dim, tiled=True)  60.4 us
    all_gather x1, waiting for transfers between devices, shards(): projected = project(lax.all_gather(inputs, 'tp', axis=0, tiled=True))  36.3 us
    dot_general x6, matrix products, project(): jnp.dot(shard_piece, matrix, preferred_element_type=jnp.float32)  14.1 us
    another operation x1, loops' own time, advance(): return lax.fori_loop(0, row_count // span_rows, one_span, states)  11.2 us
    while x1, local copies, waits for them, and re-layouts, advance(): return lax.fori_loop(0, row_count // span_rows, one_span, states)  6.32 us
    split x1, local copies, waits for them, and re-layouts, side_by_side(): jnp.split(whole, [sum(widths[:k]) for k in range(1, len(widths))], axis=a...  5.86 us
  transfers between devices with their start and end apart: 4, of which 3 were waited for; matrix products, arithmetic and copies ran while one was open for 5% of the time, Pallas kernels for 0%

commit v1 on v0

--- a/solution.py
+++ b/solution.py
@@ -117,7 +117,16 @@
             axis=1,
         )
 
-    projected = project(lax.all_gather(inputs, "tp", axis=0, tiled=True))
+    close_levels_all = lambda row_data: jnp.concatenate(
+        jax.lax.all_to_all(
+            jnp.stack([row_data for _ in range(jax.lax.axis_size("tp"))], axis=0),
+            "tp",
+            split_axis=0,
+            concat_axis=0,
+        ),
+        axis=0,
+    )
+    projected = project(close_levels_all(inputs))
     seg_rows = projected.shape[0]
     column_edges = [0]
     for matrix in matrices:

time: 290 us -> 306 us (1.055)
  blocking collectives: 0 us -> 54 us
  waiting for transfers between devices: 203 us -> 166 us
    all_to_all x0 -> x1, blocking collectives: none -> 54 us  [shards(): jax.lax.all_to_all(jnp.stack([row_data for _ in range(jax.lax.axis_size('...]
    all_gather x1 -> x0, waiting for transfers between devices: 36.3 us -> none  [shards(): projected = project(lax.all_gather(inputs, 'tp', axis=0, tiled=True))]
  transfers between devices with their start and end apart: 4 -> 3, of which waited for: 3 -> 2; matrix products, arithmetic and copies ran while one was open for 5% -> 4% of each run, Pallas kernels for 0% -> 0%
where the time goes in v1:
time: 306 us; the launch traced here: 305 us
  waiting for transfers between devices  166 us (54%)
  blocking collectives  54 us (18%)
  matrix products  25.8 us (8%)
  local copies, waits for them, and re-layouts  25.5 us (8%)
  between operations  13.7 us (4%)
  loops' own time  10.4 us (3%)
  other arithmetic  5.89 us (2%)
  starting transfers between devices  3.84 us (1%)
    reduce_scatter x1, waiting for transfers between devices, shards(): lax.psum_scatter((jnp.einsum('hqe,hen->qn', a_heads, a_weight, preferred_...  105 us
    all_gather x1, waiting for transfers between devices, side_by_side(): whole = lax.all_gather(both, axis, axis=dim, tiled=True)  60.7 us
    all_to_all x1, blocking collectives, shards(): jax.lax.all_to_all(jnp.stack([row_data for _ in range(jax.lax.axis_size('...  54 us
    dot_general x6, matrix products, project(): jnp.dot(shard_piece, matrix, preferred_element_type=jnp.float32)  11.1 us
    another operation x1, loops' own time, advance(): return lax.fori_loop(0, row_count // span_rows, one_span, states)  10.3 us
    while x1, local copies, waits for them, and re-layouts, advance(): return lax.fori_loop(0, row_count // span_rows, one_span, states)  6.32 us
  transfers between devices with their start and end apart: 3, of which 2 were waited for; matrix products, arithmetic and copies ran while one was open for 4% of the time, Pallas kernels for 0%

profile of v1, /device:TPU:0, one launch (start us, length us, event | category | flops | bytes accessed | tf_op | source)
XLA Modules:
  0.0 305.1 jit_solution(1268076111377155211)
XLA Ops:
  6.5 1.7 stack.2
  8.2 54.0 %all_to_all.5 = bf16[8,64,4096]{2,1,0:T(8,128)(2,1)S(1)} all-to-all(bf16[8,64,4096]{2,1,0:T(8,128)(2,1)S(1)} %stack.2), channel_id=1, replica_groups=mesh['sp'=16,'tp'=8] {'tp'}, dimensions={0} | all-to-all | bytes 8388608 | tf_op jit(solution)/shard_map/all_to_all | solution.py:121
  62.3 1.3 convolution_convert_fusion.2
  63.6 0.8 copy-done.1
  64.4 1.0 copy-done.10
  65.4 1.3 convolution_convert_fusion.3
  66.7 0.8 pad_maximum_fusion
  67.6 0.4 fusion.24
  68.1 3.8 %convolution_convert_fusion.4 = bf16[512,64]{0,1:T(8,128)(2,1)S(1)} fusion(bf16[512,4096]{1,0:T(8,128)(2,1)} %bitcast.108, bf16[4096,64]{0,1:T(8,128)(2,1)S(1)} %copy-done.4), kind=kOutput, calls=%fused_computation.39 | convolution fusion | flops 268468224 | bytes 4784128 | tf_op jit(solution)/shard_map/dot_general | solution.py:112
  71.9 1.4 convolution_convert_fusion.5
  73.4 3.8 %collective-permute-start = (bf16[128,128]{0,1:T(8,128)(2,1)S(1)}, bf16[128,128]{0,1:T(8,128)(2,1)S(1)}, u32[]{:S(2)}, u32[]{:S(2)}) collective-permute-start(bf16[128,128]{0,1:T(8,128)(2,1)S(1)} %pad_maximum_fusion.1), channel_id=1, source_target_pairs={{0,8},{8,16},{16,24},{24,32},{32,40},{40,48},{48,56},{56,64},{64,7... | collective-permute-start | bytes 98312 | tf_op jit(solution)/shard_map/ppermute | solution.py:18
  77.2 1.3 convolution_convert_fusion
  78.5 2.0 convolution_convert_fusion.1
  80.5 1.0 fusion.19
  81.7 1.3 fusion.20
  83.0 0.1 exponential_add_fusion
  83.0 1.8 fusion.25
  84.9 60.7 %all-gather.2.cloned.1.call-done = bf16[8192,512]{0,1:T(8,128)(2,1)} async-done(((bf16[512,512]{0,1:T(8,128)(2,1)}), bf16[8192,512]{0,1:T(8,128)(2,1)}) %all-gather.2.cloned.1.call-update) | async-done | bytes 8388624 | tf_op jit(solution)/shard_map/all_gather | solution.py:24
  145.6 5.9 %fusion.40 = (bf16[8192,256]{0,1:T(8,128)(2,1)}, bf16[8192,256]{0,1:T(8,128)(2,1)}) fusion(bf16[8192,512]{0,1:T(8,128)(2,1)} %all-gather.2.cloned.1.call-done), kind=kLoop, calls=%fused_computation.68 | loop fusion | bytes 16777216 | tf_op jit(solution)/shard_map/split | solution.py:25
  151.5 6.3 %copy.14 = bf16[8192,2,128]{2,0,1:T(8,128)(2,1)} copy(bf16[8192,2,128]{0,2,1:T(8,128)(2,1)} %bitcast.112) | data formatting | bytes 8388608 | tf_op jit(solution)/shard_map/while | solution.py:80
  157.9 29.5 %while.17 = (s32[]{:T(128)}, f32[2,2,512]{2,1,0:T(2,128)S(1)}, f32[2,2,512]{2,1,0:T(2,128)S(1)}, f32[2,2,512,128]{3,2,1,0:T(8,128)S(1)}, s32[512]{0:T(512)S(1)},...) while((s32[]{:T(128)}, f32[2,2,512]{2,1,0:T(2,128)S(1)}, ...), condition=%wide.region_5.6_spmd, body=%wide.region_0.5_spmd.sunk | while | flops 833623040 | bytes 30812476 | solution.py:80
  157.9 0.6 slice.65
  158.5 0.6 slice.64
  160.3 9.8 %conditional.2 = ((f32[2,2,512]{2,1,0:T(2,128)S(1)}, f32[2,2,512]{2,1,0:T(2,128)S(1)}, f32[2,2,512,128]{3,2,1,0:T(8,128)S(1)})) conditional(s32[]{:T(128)} %bitcast.104, (f32[2,2,512]{2,1,0:T(2,128)S(1)}, f32[2,2,512]{2,1,0:T(2,128)S(1)}, f32[2,2,512,128]{3,2,1,0:T(8,128)S(1)}) %tuple.51, (s32[512]{0:T(512)S(1)}, s32[1024]{0:T(1024)S(1)}, s32[]{:T(128)}, ...), branch_computations={%region_1.0_spmd, %region_2.4_spmd} | conditional | flops 833622016 | bytes 30808138 | solution.py:77
  160.4 0.4 broadcast_compare_fusion
  160.7 2.7 fusion
  163.5 2.1 fusion.2
  165.6 4.5 %fusion.6 = f32[2,2,512,128]{3,2,1,0:T(8,128)S(1)} fusion(f32[2,2,1024,512]{3,2,1,0:T(8,128)S(1)} %get-tuple-element.290, f32[2,2,512]{2,1,0:T(2,128)S(1)} %max.21, pred[512,1024]{0,1:T(8,128)(4,1)S(1)} %broadcast_compare_fusion, f32[2,2,512,128]{3,2,1,0:T(8,128)S(1)} %get-tuple-element.245, bf16[8192,2,128]{2,0,1:T(8,128)(2,1)} %get-tuple-element.246, ...), kind=kOutput, calls=%fused_computation.7 | convolution fusion | flops 547880960 | bytes 11550724 | tf_op jit(solution)/shard_map/while/body/eval_jaxpr/cond/branch_1_fun/hmqk,khe->hmqe/dot_general | solution.py:44
  170.1 0.6 slice.65
  170.7 0.6 slice.64
  172.6 0.6 slice.65
  173.2 0.6 slice.64
  175.1 0.6 slice.65
  175.7 0.6 slice.64
  177.5 0.6 slice.65
  178.1 0.6 slice.64
  180.0 0.6 slice.65
  180.6 0.6 slice.64
  182.5 0.6 slice.65
  183.1 0.6 slice.64
  184.9 0.6 slice.65
  185.5 0.6 slice.64
  187.4 0.3 broadcast_divide_fusion
  187.7 0.3 multiply_reduce_fusion
  188.1 1.3 fusion.30
  189.4 0.3 copy-done.3
  189.7 3.3 %fusion.18 = bf16[512,4096]{1,0:T(8,128)(2,1)} fusion(f32[512,4096,1]{1,0,2:T(8,128)S(1)} %fusion.30, bf16[512,256]{0,1:T(8,128)(2,1)S(1)} %bitcast.114, bf16[256,4096]{1,0:T(8,128)(2,1)S(1)} %copy-done.3), kind=kOutput, calls=%fused_computation.22 | convolution fusion | flops 1077936128 | bytes 14942208 | tf_op jit(solution)/shard_map/dot_general | solution.py:185
  192.9 105.3 %reduce-scatter.2.cloned.1.call-done = bf16[64,4096]{1,0:T(8,128)(2,1)} async-done(((bf16[512,4096]{1,0:T(8,128)(2,1)}), bf16[64,4096]{1,0:T(8,128)(2,1)}) %reduce-scatter.2.cloned.1.call-update) | async-done | bytes 524304 | tf_op jit(solution)/shard_map/reduce_scatter | solution.py:182
  (56 shorter events, 0.5 us)
Async XLA Ops:
  6.5 181.5 %copy-start = (bf16[256,4096]{1,0:T(8,128)(2,1)S(1)}, bf16[256,4096]{1,0:T(8,128)(2,1)}, u32[]{:S(2)}) copy-start(bf16[256,4096]{1,0:T(8,128)(2,1)} %param.26) | copy-start | bytes 6291460
  6.5 139.0 %all-gather.2.cloned.1.call-start = ((), (), s32[]{:S(2)}) async-start(), calls=%async_computation.2 | async-start | bytes 8912896 | tf_op jit(solution)/shard_map/all_gather | solution.py:24
  8.2 54.0 %copy-start.9 = (bf16[4096,256]{1,0:T(8,128)(2,1)S(1)}, bf16[4096,256]{1,0:T(8,128)(2,1)}, u32[]{:S(2)}) copy-start(bf16[4096,256]{1,0:T(8,128)(2,1)} %param.19) | copy-start | bytes 6291460
  62.3 2.1 copy-start.1
  62.3 3.1 %copy-start.10 = (bf16[4096,256]{1,0:T(8,128)(2,1)S(1)}, bf16[4096,256]{1,0:T(8,128)(2,1)}, u32[]{:S(2)}) copy-start(bf16[4096,256]{1,0:T(8,128)(2,1)} %param.18) | copy-start | bytes 6291460
  65.4 2.7 copy-start.4
  66.7 5.2 %copy-start.5 = (bf16[4096,64]{0,1:T(8,128)(2,1)S(1)}, bf16[4096,64]{0,1:T(8,128)(2,1)}, u32[]{:S(2)}) copy-start(bf16[4096,64]{0,1:T(8,128)(2,1)} %param.21) | copy-start | bytes 1572868
  67.5 230.7 %reduce-scatter.2.cloned.1.call-start = ((), (), s32[]{:S(2)}) async-start(), calls=%async_computation.3 | async-start | bytes 4718592 | tf_op jit(solution)/shard_map/reduce_scatter | solution.py:182
  67.6 4.3 %copy-start.2 = (bf16[8,64,4096]{2,1,0:T(8,128)(2,1)S(1)}, bf16[8,64,4096]{2,1,0:T(8,128)(2,1)}, u32[]{:S(2)}) copy-start(bf16[8,64,4096]{2,1,0:T(8,128)(2,1)} %copy-done.1) | copy-start | bytes 12582916
  68.1 9.1 %copy-start.11 = (bf16[4096,256]{1,0:T(8,128)(2,1)S(1)}, bf16[4096,256]{1,0:T(8,128)(2,1)}, u32[]{:S(2)}) copy-start(bf16[4096,256]{1,0:T(8,128)(2,1)} %param.20) | copy-start | bytes 6291460
  73.4 5.1 %copy-start.12 = (bf16[4096,256]{1,0:T(8,128)(2,1)S(1)}, bf16[4096,256]{1,0:T(8,128)(2,1)}, u32[]{:S(2)}) copy-start(bf16[4096,256]{1,0:T(8,128)(2,1)} %param.17) | copy-start | bytes 6291460
  73.4 7.1 %collective-permute-start = (bf16[128,128]{0,1:T(8,128)(2,1)S(1)}, bf16[128,128]{0,1:T(8,128)(2,1)S(1)}, u32[]{:S(2)}, u32[]{:S(2)}) collective-permute-start(bf16[128,128]{0,1:T(8,128)(2,1)S(1)} %pad_maximum_fusion.1), channel_id=1, source_target_pairs={{0,8},{8,16},{16,24},{24,32},{32,40},{40,48},{48,56},{56,64},{64,7... | collective-permute-start | bytes 98312 | tf_op jit(solution)/shard_map/ppermute | solution.py:18
  80.5 1.1 copy-start.8
  157.9 29.9 %copy-start.6 = (f32[2]{0:T(128)S(1)}, f32[2]{0:T(128)}, u32[]{:S(2)}) copy-start(f32[2]{0:T(128)} %param.23) | copy-start | bytes 28
  157.9 30.2 %copy-start.7 = (f32[128]{0:T(128)S(1)}, f32[128]{0:T(128)}, u32[]{:S(2)}) copy-start(f32[128]{0:T(128)} %param.24) | copy-start | bytes 1540
  188.1 1.6 copy-start.3
Sparse Core Ops, SparseCore 0:
  67.7 77.8 all-gather.1
  193.1 105.1 reduce-scatter.1
